TPU v7x, 32 devices: a whole 2x2x4 slice. The times are simulated.
32 devices in a mesh: fs: 16 (over z, y, x), tp: 2 (over core).
Axes of the slice: x: 2, y: 2, z: 4, core: 2. Of those that a mesh axis runs over, the one named last changes fastest.
Arguments:
- saved_inputs: bfloat16 [12288, 2048], P('fs'), may hold values from -8 to 8
- input_cot: bfloat16 [12288, 2048], P('fs', 'tp'), may hold values from -0.0546875 to 0.0546875
- gate_cot: bfloat16 [12288, 2048], P('fs', 'tp'), may hold values from -0.0546875 to 0.0546875
- input_master: float32 [2048, 2048], P('fs', 'tp'), may hold values from -6 to 6
- gate_master: float32 [2048, 2048], P('fs', 'tp'), may hold values from -6 to 6
- input_factor: bfloat16 [2048, 256], P('fs'), may hold values from -2 to 2
- gate_factor: bfloat16 [2048, 256], P('fs'), may hold values from -2 to 2
- input_first: float32 [256, 2048], P('fs', 'tp'), may hold values from -6 to 6
- input_second: float32 [256, 2048], P('fs', 'tp'), may hold values from 0.2 to 17
- gate_first: float32 [256, 2048], P('fs', 'tp'), may hold values from -6 to 6
- gate_second: float32 [256, 2048], P('fs', 'tp'), may hold values from 0.2 to 17
Outputs:
- input_step: float32 [2048, 2048], P('fs', 'tp')
- gate_step: float32 [2048, 2048], P('fs', 'tp')
- input_first_new: float32 [256, 2048], P('fs', 'tp')
- input_second_new: float32 [256, 2048], P('fs', 'tp')
- gate_first_new: float32 [256, 2048], P('fs', 'tp')
- gate_second_new: float32 [256, 2048], P('fs', 'tp')
- input_copy: bfloat16 [2048, 2048], P(None, 'tp')
- gate_copy: bfloat16 [2048, 2048], P(None, 'tp')
All inputs are finite; a program needn't handle non-finite values.
Results may differ from a plain program's by a relative error of at most 0.0004.
Values may be sent and summed in bfloat16 or wider, within the bound.
A program may use at most 64 MiB of HBM per device.

v0:
```python
import jax
import jax.numpy as jnp
from jax import lax
from jax.sharding import PartitionSpec as P

D = 2048
W = 2048
first_decay = 0.9
second_decay = 0.9
ratio_floor = 1e-08
mean_floor = 1e-06
step_size = 0.05


def moments(low_rank, first, second):
    first_new = first_decay * first + (1.0 - first_decay) * low_rank
    second_new = second_decay * second + (1.0 - second_decay) * low_rank * low_rank
    ratio = first_new / (jnp.sqrt(second_new) + ratio_floor)
    return (first_new, second_new, ratio)


def local(
    saved_inputs,
    input_cot,
    gate_cot,
    input_master,
    gate_master,
    input_factor,
    gate_factor,
    input_first,
    input_second,
    gate_first,
    gate_second,
):
    col_width = input_cot.shape[1]
    contract = (((0,), (0,)), ((), ()))
    factor_in = input_factor.astype(jnp.float32)
    factor_gate = gate_factor.astype(jnp.float32)
    whole_in, whole_gate = (
        lax.all_gather(input_factor, "fs", axis=0, tiled=True),
        lax.all_gather(gate_factor, "fs", axis=0, tiled=True),
    )
    partial_in = lax.dot_general(
        saved_inputs, input_cot, contract, preferred_element_type=jnp.float32
    )
    partial_gate = lax.dot_general(
        saved_inputs, gate_cot, contract, preferred_element_type=jnp.float32
    )
    cols_in = whole_in.astype(jnp.float32)
    cols_gate = whole_gate.astype(jnp.float32)
    term_in = lax.dot_general(cols_in, partial_in, contract, precision=lax.Precision.HIGHEST)
    term_gate = lax.dot_general(cols_gate, partial_gate, contract, precision=lax.Precision.HIGHEST)
    summed = lax.psum_scatter(
        jnp.concatenate([term_in, term_gate], axis=1), "fs", scatter_dimension=0, tiled=True
    )
    low_in = summed[:, :col_width]
    low_gate = summed[:, col_width:]
    first_in, second_in, ratio_in = moments(low_in, input_first, input_second)
    first_gate, second_gate, ratio_gate = moments(low_gate, gate_first, gate_second)
    piece_in = lax.all_gather(ratio_in, "fs", axis=0, tiled=True)
    piece_gate = lax.all_gather(ratio_gate, "fs", axis=0, tiled=True)
    cols_in = factor_in
    cols_gate = factor_gate
    dir_in = jnp.dot(cols_in, piece_in, precision=lax.Precision.HIGHEST)
    dir_gate = jnp.dot(cols_gate, piece_gate, precision=lax.Precision.HIGHEST)
    square_in, square_gate = lax.psum(
        (jnp.sum(dir_in * dir_in), jnp.sum(dir_gate * dir_gate)), ("fs", "tp")
    )
    step_in = dir_in * lax.rsqrt(square_in / (D * W) + mean_floor)
    step_gate = dir_gate * lax.rsqrt(square_gate / (D * W) + mean_floor)
    local_in = (input_master - step_size * step_in).astype(jnp.bfloat16)
    local_gate = (gate_master - step_size * step_gate).astype(jnp.bfloat16)
    copy_in, copy_gate = (
        lax.all_gather(local_in, "fs", axis=0, tiled=True),
        lax.all_gather(local_gate, "fs", axis=0, tiled=True),
    )
    return (step_in, step_gate, first_in, second_in, first_gate, second_gate, copy_in, copy_gate)


def solution(mesh):
    return jax.shard_map(
        local,
        mesh=mesh,
        in_specs=(
            P("fs", None),
            P("fs", "tp"),
            P("fs", "tp"),
            P("fs", "tp"),
            P("fs", "tp"),
            P("fs", None),
            P("fs", None),
            P("fs", "tp"),
            P("fs", "tp"),
            P("fs", "tp"),
            P("fs", "tp"),
        ),
        out_specs=(
            P("fs", "tp"),
            P("fs", "tp"),
            P("fs", "tp"),
            P("fs", "tp"),
            P("fs", "tp"),
            P("fs", "tp"),
            P(None, "tp"),
            P(None, "tp"),
        ),
        check_vma=False,
    )
```

profile of v0, /device:TPU:0, one launch (start us, length us, event | category | flops | bytes accessed | tf_op | source)
XLA Modules:
  0.0 569.3 jit_solution(10387800890137530023)
XLA Ops:
  7.2 0.0 copy-start
  7.2 0.0 all-gather.7.cloned.1.call-start
  7.2 0.7 all-gather.7.cloned.1.call-update
  7.9 0.0 all-gather.9.cloned.1.call-start
  8.0 0.7 all-gather.9.cloned.1.call-update
  8.7 0.0 reduce-scatter.4.cloned.1.call-start
  8.7 0.3 copy-done
  9.1 7.2 %fusion.4 = f32[2048,1024]{1,0:T(8,128)} fusion(bf16[768,2048]{1,0:T(8,128)(2,1)S(1)} %copy-done, bf16[768,1024]{1,0:T(8,128)(2,1)} %param.12), kind=kOutput, calls=%fused_computation.17 | convolution fusion | flops 3221225472 | bytes 13107200 | tf_op jit(solution)/shard_map/dot_general | solution.py:43
  16.2 0.0 copy-done.8
  16.2 5.7 %fusion.5 = f32[2048,1024]{1,0:T(8,128)} fusion(bf16[768,2048]{1,0:T(8,128)(2,1)S(1)} %copy-done, bf16[768,1024]{1,0:T(8,128)(2,1)S(1)} %copy-done.8), kind=kOutput, calls=%fused_computation.18 | convolution fusion | flops 3221225472 | bytes 13107200 | tf_op jit(solution)/shard_map/dot_general | solution.py:46
  21.9 46.7 %all-gather.7.cloned.1.call-done = bf16[2048,256]{1,0:T(8,128)(2,1)} async-done(((bf16[128,256]{1,0:T(8,128)(2,1)}), bf16[2048,256]{1,0:T(8,128)(2,1)}) %all-gather.7.cloned.1.call-update) | async-done | bytes 1048592 | tf_op jit(solution)/shard_map/all_gather | solution.py:40
  68.6 11.2 %convolution_bitcast_fusion.1 = f32[256,1024]{0,1:T(8,128)} fusion(f32[2048,1024]{1,0:T(8,128)} %fusion.4, bf16[2048,256]{1,0:T(8,128)(2,1)} %all-gather.7.cloned.1.call-done), kind=kOutput, calls=%fused_computation.2 | convolution fusion | flops 6442450944 | bytes 10485760 | tf_op jit(solution)/shard_map/dot_general | solution.py:51
  79.8 45.5 %all-gather.9.cloned.1.call-done = bf16[2048,256]{1,0:T(8,128)(2,1)} async-done(((bf16[128,256]{1,0:T(8,128)(2,1)}), bf16[2048,256]{1,0:T(8,128)(2,1)}) %all-gather.9.cloned.1.call-update) | async-done | bytes 1048592 | tf_op jit(solution)/shard_map/all_gather | solution.py:41
  125.3 9.5 %convolution_bitcast_fusion = f32[256,1024]{0,1:T(8,128)S(1)} fusion(f32[2048,1024]{1,0:T(8,128)} %fusion.5, bf16[2048,256]{1,0:T(8,128)(2,1)} %all-gather.9.cloned.1.call-done), kind=kOutput, calls=%fused_computation.1 | convolution fusion | flops 6442450944 | bytes 10485760 | tf_op jit(solution)/shard_map/dot_general | solution.py:52
  134.8 0.0 copy-done.1
  134.8 1.5 pad_maximum_fusion
  136.2 0.0 copy-start.2
  136.3 2.9 copy.65
  139.2 0.0 reduce-scatter.4.cloned.1.call-update
  139.2 0.0 all-gather.13.cloned.1.call-start
  139.3 80.6 %reduce-scatter.4.cloned.1.call-done = f32[16,2048]{1,0:T(8,128)} async-done(((f32[256,2048]{1,0:T(8,128)}), f32[16,2048]{1,0:T(8,128)}) %reduce-scatter.4.cloned.1.call-update) | async-done | bytes 131088 | tf_op jit(solution)/shard_map/reduce_scatter | solution.py:53
  219.9 0.0 copy-done.4
  219.9 0.0 copy-done.5
  219.9 0.0 copy-done.6
  219.9 0.0 copy-done.7
  219.9 1.6 add_divide_fusion
  221.5 0.0 all-gather.13.cloned.1.call-update
  221.5 0.0 all-gather.11.cloned.1.call-start
  221.6 0.5 all-gather.11.cloned.1.call-update
  222.1 0.0 all-gather.15.cloned.1.call-start
  222.2 2.0 copy.59
  224.2 50.4 %all-gather.13.cloned.1.call-done = f32[256,1024]{1,0:T(8,128)} async-done(((f32[16,1024]{1,0:T(8,128)}), f32[256,1024]{1,0:T(8,128)}) %all-gather.13.cloned.1.call-update) | async-done | bytes 1048592 | tf_op jit(solution)/shard_map/all_gather | solution.py:61
  274.6 3.7 multiply_reduce_fusion
  278.3 53.4 %all-gather.11.cloned.1.call-done = f32[256,1024]{1,0:T(8,128)} async-done(((f32[16,1024]{1,0:T(8,128)}), f32[256,1024]{1,0:T(8,128)}) %all-gather.11.cloned.1.call-update) | async-done | bytes 1048592 | tf_op jit(solution)/shard_map/all_gather | solution.py:60
  331.7 3.6 multiply_reduce_fusion.1
  335.4 38.6 %all-reduce = (f32[]{:T(128)}, f32[]{:T(128)}) all-reduce(f32[]{:T(128)} %get-tuple-element.47, f32[]{:T(128)} %get-tuple-element.49), channel_id=1, replica_groups=mesh['fs'=16,'tp'=2] {'fs','tp'}, use_global_device_ids=true, to_apply=%region_2.0 | all-reduce | flops 2 | bytes 16 | tf_op jit(solution)/shard_map/psum | solution.py:66
  374.7 2.2 subtract_convert_fusion.1
  376.8 0.0 all-gather.15.cloned.1.call-update
  376.9 0.0 all-gather.17.cloned.1.call-start
  376.9 2.0 copy.60
  379.7 2.2 subtract_convert_fusion
  381.8 0.0 all-gather.17.cloned.1.call-update
  381.9 2.0 copy.61
  383.9 2.0 copy.62
  385.9 80.5 %all-gather.15.cloned.1.call-done = bf16[2048,1024]{0,1:T(8,128)(2,1)} async-done(((bf16[128,1024]{0,1:T(8,128)(2,1)}), bf16[2048,1024]{0,1:T(8,128)(2,1)}) %all-gather.15.cloned.1.call-update) | async-done | bytes 4194320 | tf_op jit(solution)/shard_map/all_gather | solution.py:74
  466.4 6.4 %copy.63 = bf16[2048,1024]{1,0:T(8,128)(2,1)} copy(bf16[2048,1024]{0,1:T(8,128)(2,1)} %all-gather.15.cloned.1.call-done) | data formatting | bytes 8388608
  472.8 83.2 %all-gather.17.cloned.1.call-done = bf16[2048,1024]{0,1:T(8,128)(2,1)} async-done(((bf16[128,1024]{0,1:T(8,128)(2,1)}), bf16[2048,1024]{0,1:T(8,128)(2,1)}) %all-gather.17.cloned.1.call-update) | async-done | bytes 4194320 | tf_op jit(solution)/shard_map/all_gather | solution.py:75
  556.0 6.4 %copy.64 = bf16[2048,1024]{1,0:T(8,128)(2,1)} copy(bf16[2048,1024]{0,1:T(8,128)(2,1)} %all-gather.17.cloned.1.call-done) | data formatting | bytes 8388608
  (9 shorter events, 0.0 us)
Async XLA Ops:
  7.2 1.9 copy-start
  7.2 61.4 %all-gather.7.cloned.1.call-start = ((), (), s32[]{:S(2)}) async-start(), calls=%async_computation.1 | async-start | bytes 1114112 | tf_op jit(solution)/shard_map/all_gather | solution.py:40
  7.9 117.4 %all-gather.9.cloned.1.call-start = ((), (), s32[]{:S(2)}) async-start(), calls=%async_computation.2 | async-start | bytes 1114112 | tf_op jit(solution)/shard_map/all_gather | solution.py:41
  8.7 211.2 %reduce-scatter.4.cloned.1.call-start = ((), (), s32[]{:S(2)}) async-start(), calls=%async_computation.7 | async-start | bytes 2228224 | tf_op jit(solution)/shard_map/reduce_scatter | solution.py:53
  9.1 7.2 %copy-start.8 = (bf16[768,1024]{1,0:T(8,128)(2,1)S(1)}, bf16[768,1024]{1,0:T(8,128)(2,1)}, u32[]{:S(2)}) copy-start(bf16[768,1024]{1,0:T(8,128)(2,1)} %param.13) | copy-start | bytes 4718596
  125.3 9.5 %copy-start.1 = (f32[256,1024]{0,1:T(8,128)S(1)}, f32[256,1024]{0,1:T(8,128)}, u32[]{:S(2)}) copy-start(f32[256,1024]{0,1:T(8,128)} %convolution_bitcast_fusion.1) | copy-start | bytes 3145732
  136.2 83.6 %copy-start.4 = (f32[16,1024]{1,0:T(8,128)S(1)}, f32[16,1024]{1,0:T(8,128)}, u32[]{:S(2)}) copy-start(f32[16,1024]{1,0:T(8,128)} %param.21) | copy-start | bytes 196612
  136.2 83.6 %copy-start.5 = (f32[16,1024]{1,0:T(8,128)S(1)}, f32[16,1024]{1,0:T(8,128)}, u32[]{:S(2)}) copy-start(f32[16,1024]{1,0:T(8,128)} %param.20) | copy-start | bytes 196612
  136.2 83.6 %copy-start.6 = (f32[16,1024]{1,0:T(8,128)S(1)}, f32[16,1024]{1,0:T(8,128)}, u32[]{:S(2)}) copy-start(f32[16,1024]{1,0:T(8,128)} %param.19) | copy-start | bytes 196612
  136.2 83.6 %copy-start.7 = (f32[16,1024]{1,0:T(8,128)S(1)}, f32[16,1024]{1,0:T(8,128)}, u32[]{:S(2)}) copy-start(f32[16,1024]{1,0:T(8,128)} %param.18) | copy-start | bytes 196612
  136.2 138.3 %copy-start.2 = (bf16[128,256]{1,0:T(8,128)(2,1)S(1)}, bf16[128,256]{1,0:T(8,128)(2,1)}, u32[]{:S(2)}) copy-start(bf16[128,256]{1,0:T(8,128)(2,1)} %param.17) | copy-start | bytes 196612
  139.2 192.5 %copy-start.3 = (bf16[128,256]{1,0:T(8,128)(2,1)S(1)}, bf16[128,256]{1,0:T(8,128)(2,1)}, u32[]{:S(2)}) copy-start(bf16[128,256]{1,0:T(8,128)(2,1)} %param.16) | copy-start | bytes 196612
  139.2 135.4 %all-gather.13.cloned.1.call-start = ((), (), s32[]{:S(2)}) async-start(), calls=%async_computation.4 | async-start | bytes 1114112 | tf_op jit(solution)/shard_map/all_gather | solution.py:61
  221.5 110.2 %all-gather.11.cloned.1.call-start = ((), (), s32[]{:S(2)}) async-start(), calls=%async_computation.3 | async-start | bytes 1114112 | tf_op jit(solution)/shard_map/all_gather | solution.py:60
  222.1 244.3 %all-gather.15.cloned.1.call-start = ((), (), s32[]{:S(2)}) async-start(), calls=%async_computation.5 | async-start | bytes 4456448 | tf_op jit(solution)/shard_map/all_gather | solution.py:74
  376.9 179.2 %all-gather.17.cloned.1.call-start = ((), (), s32[]{:S(2)}) async-start(), calls=%async_computation.6 | async-start | bytes 4456448 | tf_op jit(solution)/shard_map/all_gather | solution.py:75
Sparse Core Ops, SparseCore 0:
  10.7 57.7 all-gather.6
  71.3 53.9 all-gather.8
  139.3 80.4 reduce-scatter.3
  223.0 51.4 all-gather.12
  277.8 53.9 all-gather.10
  377.0 89.3 all-gather.14
  469.1 86.8 all-gather.16
where the time goes:
time: 570 us; the launch traced here: 569 us
  waiting for transfers between devices  442 us (78%)
  matrix products  40.9 us (7%)
  blocking collectives  38.6 us (7%)
  local copies, waits for them, and re-layouts  24.2 us (4%)
  between operations  15.6 us (3%)
  other arithmetic  7.42 us (1%)
    all_gather x1, waiting for transfers between devices, local(): lax.all_gather(local_gate, 'fs', axis=0, tiled=True)  83.2 us
    reduce_scatter x1, waiting for transfers between devices, local(): lax.psum_scatter(jnp.concatenate([term_in, term_gate], axis=1), 'fs', sca...  80.6 us
    all_gather x1, waiting for transfers between devices, local(): lax.all_gather(local_in, 'fs', axis=0, tiled=True)  80.5 us
    all_gather x1, waiting for transfers between devices, local(): piece_in = lax.all_gather(ratio_in, 'fs', axis=0, tiled=True)  53.4 us
    all_gather x1, waiting for transfers between devices, local(): piece_gate = lax.all_gather(ratio_gate, 'fs', axis=0, tiled=True)  50.4 us
    all_gather x1, waiting for transfers between devices, local(): lax.all_gather(input_factor, 'fs', axis=0, tiled=True)  46.7 us
    all_gather x1, waiting for transfers between devices, local(): lax.all_gather(gate_factor, 'fs', axis=0, tiled=True)  45.5 us
    psum x1, blocking collectives, local(): lax.psum((jnp.sum(dir_in * dir_in), jnp.sum(dir_gate * dir_gate)), ('fs',...  38.6 us
  transfers between devices with their start and end apart: 7, of which 7 were waited for; matrix products, arithmetic and copies ran while one was open for 8% of the time, Pallas kernels for 0%

commit v1 on v0

--- a/solution.py
+++ b/solution.py
@@ -58,7 +58,12 @@
     first_in, second_in, ratio_in = moments(low_in, input_first, input_second)
     first_gate, second_gate, ratio_gate = moments(low_gate, gate_first, gate_second)
     piece_in = lax.all_gather(ratio_in, "fs", axis=0, tiled=True)
-    piece_gate = lax.all_gather(ratio_gate, "fs", axis=0, tiled=True)
+    ring = [ratio_gate]
+    for hop in range(15):
+        ring.append(lax.ppermute(ring[-1], "fs", [(dev, (dev + 1) % 16) for dev in range(16)]))
+    piece_gate = jnp.roll(
+        jnp.concatenate(ring[::-1], axis=0), (lax.axis_index("fs") + 1) * ring[0].shape[0], axis=0
+    )
     cols_in = factor_in
     cols_gate = factor_gate
     dir_in = jnp.dot(cols_in, piece_in, precision=lax.Precision.HIGHEST)

time: 570 us -> 635 us (1.11)
  waiting for transfers between devices: 442 us -> 491 us
  local copies, waits for them, and re-layouts: 24.2 us -> 41.2 us
    ppermute x0 -> x15, waiting for transfers between devices: none -> 117 us  [local(): lax.ppermute(ring[-1], 'fs', [(dev, (dev + 1) % 16) for dev in range(16)])]
    all_gather x1 -> x0, waiting for transfers between devices: 50.4 us -> none  [local(): piece_gate = lax.all_gather(ratio_gate, 'fs', axis=0, tiled=True)]
    all_gather x1, waiting for transfers between devices: 53.4 us -> 35.9 us  [local(): piece_in = lax.all_gather(ratio_in, 'fs', axis=0, tiled=True)]
    unnamed x25 -> x94, local copies, waits for them, and re-layouts: 24.2 us -> 41.2 us
  transfers between devices with their start and end apart: 7 -> 21, of which waited for: 7 -> 21; matrix products, arithmetic and copies ran while one was open for 8% -> 9% of each run, Pallas kernels for 0% -> 0%
where the time goes in v1:
time: 635 us; the launch traced here: 634 us
  waiting for transfers between devices  491 us (77%)
  local copies, waits for them, and re-layouts  41.2 us (6%)
  matrix products  39.6 us (6%)
  blocking collectives  38.6 us (6%)
  between operations  15.9 us (3%)
  other arithmetic  7.41 us (1%)
    ppermute x15, waiting for transfers between devices, local(): lax.ppermute(ring[-1], 'fs', [(dev, (dev + 1) % 16) for dev in range(16)])  117 us
    all_gather x1, waiting for transfers between devices, local(): lax.all_gather(local_gate, 'fs', axis=0, tiled=True)  83.1 us
    reduce_scatter x1, waiting for transfers between devices, local(): lax.psum_scatter(jnp.concatenate([term_in, term_gate], axis=1), 'fs', sca...  80.6 us
    all_gather x1, waiting for transfers between devices, local(): lax.all_gather(local_in, 'fs', axis=0, tiled=True)  80.5 us
    all_gather x1, waiting for transfers between devices, local(): lax.all_gather(input_factor, 'fs', axis=0, tiled=True)  46.7 us
    all_gather x1, waiting for transfers between devices, local(): lax.all_gather(gate_factor, 'fs', axis=0, tiled=True)  45.5 us
    unnamed x94, local copies, waits for them, and re-layouts  41.2 us
    psum x1, blocking collectives, local(): lax.psum((jnp.sum(dir_in * dir_in), jnp.sum(dir_gate * dir_gate)), ('fs',...  38.6 us
  transfers between devices with their start and end apart: 21, of which 21 were waited for; matrix products, arithmetic and copies ran while one was open for 9% of the time, Pallas kernels for 0%

profile of v1, /device:TPU:0, one launch (start us, length us, event | category | flops | bytes accessed | tf_op | source)
XLA Modules:
  0.0 633.6 jit_solution(2017384833539791759)
XLA Ops:
  9.1 7.1 %fusion.7 = f32[2048,1024]{1,0:T(8,128)} fusion(bf16[768,2048]{1,0:T(8,128)(2,1)S(1)} %copy-done, bf16[768,1024]{1,0:T(8,128)(2,1)} %param.12), kind=kOutput, calls=%fused_computation.52 | convolution fusion | flops 3221225472 | bytes 13107200 | tf_op jit(solution)/shard_map/dot_general | solution.py:43
  16.2 5.7 fusion.8
  21.9 46.7 %all-gather.6.cloned.1.call-done = bf16[2048,256]{1,0:T(8,128)(2,1)} async-done(((bf16[128,256]{1,0:T(8,128)(2,1)}), bf16[2048,256]{1,0:T(8,128)(2,1)}) %all-gather.6.cloned.1.call-update) | async-done | bytes 1048592 | tf_op jit(solution)/shard_map/all_gather | solution.py:40
  68.6 11.2 %convolution_bitcast_fusion.1 = f32[256,1024]{0,1:T(8,128)} fusion(f32[2048,1024]{1,0:T(8,128)} %fusion.7, bf16[2048,256]{1,0:T(8,128)(2,1)} %all-gather.6.cloned.1.call-done), kind=kOutput, calls=%fused_computation.2 | convolution fusion | flops 6442450944 | bytes 10485760 | tf_op jit(solution)/shard_map/dot_general | solution.py:51
  79.8 45.5 %all-gather.8.cloned.1.call-done = bf16[2048,256]{1,0:T(8,128)(2,1)} async-done(((bf16[128,256]{1,0:T(8,128)(2,1)}), bf16[2048,256]{1,0:T(8,128)(2,1)}) %all-gather.8.cloned.1.call-update) | async-done | bytes 1048592 | tf_op jit(solution)/shard_map/all_gather | solution.py:41
  125.3 9.5 %convolution_bitcast_fusion = f32[256,1024]{0,1:T(8,128)S(1)} fusion(f32[2048,1024]{1,0:T(8,128)} %fusion.8, bf16[2048,256]{1,0:T(8,128)(2,1)} %all-gather.8.cloned.1.call-done), kind=kOutput, calls=%fused_computation.1 | convolution fusion | flops 6442450944 | bytes 10485760 | tf_op jit(solution)/shard_map/dot_general | solution.py:52
  134.8 1.5 pad_maximum_fusion
  136.2 2.9 copy.64
  139.2 80.6 %reduce-scatter.4.cloned.1.call-done = f32[16,2048]{1,0:T(8,128)} async-done(((f32[256,2048]{1,0:T(8,128)}), f32[16,2048]{1,0:T(8,128)}) %reduce-scatter.4.cloned.1.call-update) | async-done | bytes 131088 | tf_op jit(solution)/shard_map/reduce_scatter | solution.py:53
  219.8 1.6 add_divide_fusion
  221.4 7.9 %collective-permute-done = f32[16,1024]{1,0:T(8,128)S(1)} collective-permute-done((f32[16,1024]{1,0:T(8,128)S(1)}, f32[16,1024]{1,0:T(8,128)S(1)}, u32[]{:S(2)}, u32[]{:S(2)}) %collective-permute-start) | collective-permute-done | bytes 65568 | tf_op jit(solution)/shard_map/ppermute | solution.py:63
  229.3 8.5 %collective-permute-done.1 = f32[16,1024]{1,0:T(8,128)S(1)} collective-permute-done((f32[16,1024]{1,0:T(8,128)S(1)}, f32[16,1024]{1,0:T(8,128)S(1)}, u32[]{:S(2)}, u32[]{:S(2)}) %collective-permute-start.1) | collective-permute-done | bytes 65568 | tf_op jit(solution)/shard_map/ppermute | solution.py:63
  237.8 7.9 %collective-permute-done.2 = f32[16,1024]{1,0:T(8,128)S(1)} collective-permute-done((f32[16,1024]{1,0:T(8,128)S(1)}, f32[16,1024]{1,0:T(8,128)S(1)}, u32[]{:S(2)}, u32[]{:S(2)}) %collective-permute-start.2) | collective-permute-done | bytes 65568 | tf_op jit(solution)/shard_map/ppermute | solution.py:63
  245.6 7.9 %collective-permute-done.3 = f32[16,1024]{1,0:T(8,128)S(1)} collective-permute-done((f32[16,1024]{1,0:T(8,128)S(1)}, f32[16,1024]{1,0:T(8,128)S(1)}, u32[]{:S(2)}, u32[]{:S(2)}) %collective-permute-start.3) | collective-permute-done | bytes 65568 | tf_op jit(solution)/shard_map/ppermute | solution.py:63
  253.5 7.9 %collective-permute-done.4 = f32[16,1024]{1,0:T(8,128)S(1)} collective-permute-done((f32[16,1024]{1,0:T(8,128)S(1)}, f32[16,1024]{1,0:T(8,128)S(1)}, u32[]{:S(2)}, u32[]{:S(2)}) %collective-permute-start.4) | collective-permute-done | bytes 65568 | tf_op jit(solution)/shard_map/ppermute | solution.py:63
  261.4 7.9 %collective-permute-done.5 = f32[16,1024]{1,0:T(8,128)S(1)} collective-permute-done((f32[16,1024]{1,0:T(8,128)S(1)}, f32[16,1024]{1,0:T(8,128)S(1)}, u32[]{:S(2)}, u32[]{:S(2)}) %collective-permute-start.5) | collective-permute-done | bytes 65568 | tf_op jit(solution)/shard_map/ppermute | solution.py:63
  269.8 7.9 %collective-permute-done.6 = f32[16,1024]{1,0:T(8,128)S(1)} collective-permute-done((f32[16,1024]{1,0:T(8,128)S(1)}, f32[16,1024]{1,0:T(8,128)S(1)}, u32[]{:S(2)}, u32[]{:S(2)}) %collective-permute-start.6) | collective-permute-done | bytes 65568 | tf_op jit(solution)/shard_map/ppermute | solution.py:63
  278.3 7.9 %collective-permute-done.7 = f32[16,1024]{1,0:T(8,128)S(1)} collective-permute-done((f32[16,1024]{1,0:T(8,128)S(1)}, f32[16,1024]{1,0:T(8,128)S(1)}, u32[]{:S(2)}, u32[]{:S(2)}) %collective-permute-start.7) | collective-permute-done | bytes 65568 | tf_op jit(solution)/shard_map/ppermute | solution.py:63
  286.8 7.9 %collective-permute-done.8 = f32[16,1024]{1,0:T(8,128)S(1)} collective-permute-done((f32[16,1024]{1,0:T(8,128)S(1)}, f32[16,1024]{1,0:T(8,128)S(1)}, u32[]{:S(2)}, u32[]{:S(2)}) %collective-permute-start.8) | collective-permute-done | bytes 65568 | tf_op jit(solution)/shard_map/ppermute | solution.py:63
  295.3 8.2 %collective-permute-done.9 = f32[16,1024]{1,0:T(8,128)S(1)} collective-permute-done((f32[16,1024]{1,0:T(8,128)S(1)}, f32[16,1024]{1,0:T(8,128)S(1)}, u32[]{:S(2)}, u32[]{:S(2)}) %collective-permute-start.9) | collective-permute-done | bytes 65568 | tf_op jit(solution)/shard_map/ppermute | solution.py:63
  304.1 7.9 %collective-permute-done.10 = f32[16,1024]{1,0:T(8,128)S(1)} collective-permute-done((f32[16,1024]{1,0:T(8,128)S(1)}, f32[16,1024]{1,0:T(8,128)S(1)}, u32[]{:S(2)}, u32[]{:S(2)}) %collective-permute-start.10) | collective-permute-done | bytes 65568 | tf_op jit(solution)/shard_map/ppermute | solution.py:63
  312.6 7.9 %collective-permute-done.11 = f32[16,1024]{1,0:T(8,128)S(1)} collective-permute-done((f32[16,1024]{1,0:T(8,128)S(1)}, f32[16,1024]{1,0:T(8,128)S(1)}, u32[]{:S(2)}, u32[]{:S(2)}) %collective-permute-start.11) | collective-permute-done | bytes 65568 | tf_op jit(solution)/shard_map/ppermute | solution.py:63
  321.1 7.9 %collective-permute-done.12 = f32[16,1024]{1,0:T(8,128)S(1)} collective-permute-done((f32[16,1024]{1,0:T(8,128)S(1)}, f32[16,1024]{1,0:T(8,128)S(1)}, u32[]{:S(2)}, u32[]{:S(2)}) %collective-permute-start.12) | collective-permute-done | bytes 65568 | tf_op jit(solution)/shard_map/ppermute | solution.py:63
  329.6 8.0 %collective-permute-done.13 = f32[16,1024]{1,0:T(8,128)} collective-permute-done((f32[16,1024]{1,0:T(8,128)S(1)}, f32[16,1024]{1,0:T(8,128)}, u32[]{:S(2)}, u32[]{:S(2)}) %collective-permute-start.13) | collective-permute-done | bytes 65568 | tf_op jit(solution)/shard_map/ppermute | solution.py:63
  337.6 2.0 copy.58
  339.8 6.0 collective-permute-done.14
  345.7 0.8 constant_dynamic-update-slice_fusion.31
  346.6 0.8 constant_dynamic-update-slice_fusion.30
  348.3 0.8 constant_dynamic-update-slice_fusion.28
  349.1 0.8 constant_dynamic-update-slice_fusion.27
  350.0 0.8 constant_dynamic-update-slice_fusion.26
  352.5 0.8 constant_dynamic-update-slice_fusion.23
  353.3 0.8 constant_dynamic-update-slice_fusion.22
  355.1 0.8 constant_dynamic-update-slice_fusion.15
  357.0 0.8 constant_dynamic-update-slice_fusion.4
  357.9 2.4 multiply_reduce_fusion
  360.4 35.9 %all-gather.10.cloned.1.call-done = f32[256,1024]{1,0:T(8,128)} async-done(((f32[16,1024]{1,0:T(8,128)}), f32[256,1024]{1,0:T(8,128)}) %all-gather.10.cloned.1.call-update) | async-done | bytes 1048592 | tf_op jit(solution)/shard_map/all_gather | solution.py:60
  396.3 3.6 multiply_reduce_fusion.1
  399.9 38.6 %all-reduce = (f32[]{:T(128)}, f32[]{:T(128)}) all-reduce(f32[]{:T(128)} %get-tuple-element.47, f32[]{:T(128)} %get-tuple-element.49), channel_id=1, replica_groups=mesh['fs'=16,'tp'=2] {'fs','tp'}, use_global_device_ids=true, to_apply=%region_2.3 | all-reduce | flops 2 | bytes 16 | tf_op jit(solution)/shard_map/psum | solution.py:71
  439.2 2.2 subtract_convert_fusion.1
  441.4 2.0 copy.59
  444.1 2.2 subtract_convert_fusion
  446.3 2.0 copy.60
  448.4 2.0 copy.61
  450.4 80.5 %all-gather.12.cloned.1.call-done = bf16[2048,1024]{0,1:T(8,128)(2,1)} async-done(((bf16[128,1024]{0,1:T(8,128)(2,1)}), bf16[2048,1024]{0,1:T(8,128)(2,1)}) %all-gather.12.cloned.1.call-update) | async-done | bytes 4194320 | tf_op jit(solution)/shard_map/all_gather | solution.py:79
  530.9 6.4 %copy.62 = bf16[2048,1024]{1,0:T(8,128)(2,1)} copy(bf16[2048,1024]{0,1:T(8,128)(2,1)} %all-gather.12.cloned.1.call-done) | data formatting | bytes 8388608
  537.3 83.1 %all-gather.14.cloned.1.call-done = bf16[2048,1024]{0,1:T(8,128)(2,1)} async-done(((bf16[128,1024]{0,1:T(8,128)(2,1)}), bf16[2048,1024]{0,1:T(8,128)(2,1)}) %all-gather.14.cloned.1.call-update) | async-done | bytes 4194320 | tf_op jit(solution)/shard_map/all_gather | solution.py:80
  620.4 6.4 %copy.63 = bf16[2048,1024]{1,0:T(8,128)(2,1)} copy(bf16[2048,1024]{0,1:T(8,128)(2,1)} %all-gather.14.cloned.1.call-done) | data formatting | bytes 8388608
  (106 shorter events, 11.5 us)
Async XLA Ops:
  7.2 1.9 copy-start
  7.2 61.4 %all-gather.6.cloned.1.call-start = ((), (), s32[]{:S(2)}) async-start(), calls=%async_computation.1 | async-start | bytes 1114112 | tf_op jit(solution)/shard_map/all_gather | solution.py:40
  7.9 117.4 %all-gather.8.cloned.1.call-start = ((), (), s32[]{:S(2)}) async-start(), calls=%async_computation.2 | async-start | bytes 1114112 | tf_op jit(solution)/shard_map/all_gather | solution.py:41
  8.7 211.1 %reduce-scatter.4.cloned.1.call-start = ((), (), s32[]{:S(2)}) async-start(), calls=%async_computation.6 | async-start | bytes 2228224 | tf_op jit(solution)/shard_map/reduce_scatter | solution.py:53
  9.1 7.2 %copy-start.27 = (bf16[768,1024]{1,0:T(8,128)(2,1)S(1)}, bf16[768,1024]{1,0:T(8,128)(2,1)}, u32[]{:S(2)}) copy-start(bf16[768,1024]{1,0:T(8,128)(2,1)} %param.13) | copy-start | bytes 4718596
  125.3 9.5 %copy-start.1 = (f32[256,1024]{0,1:T(8,128)S(1)}, f32[256,1024]{0,1:T(8,128)}, u32[]{:S(2)}) copy-start(f32[256,1024]{0,1:T(8,128)} %convolution_bitcast_fusion.1) | copy-start | bytes 3145732
  139.1 80.7 %copy-start.23 = (f32[16,1024]{1,0:T(8,128)S(1)}, f32[16,1024]{1,0:T(8,128)}, u32[]{:S(2)}) copy-start(f32[16,1024]{1,0:T(8,128)} %param.21) | copy-start | bytes 196612
  139.1 80.7 %copy-start.24 = (f32[16,1024]{1,0:T(8,128)S(1)}, f32[16,1024]{1,0:T(8,128)}, u32[]{:S(2)}) copy-start(f32[16,1024]{1,0:T(8,128)} %param.20) | copy-start | bytes 196612
  139.1 80.7 %copy-start.25 = (f32[16,1024]{1,0:T(8,128)S(1)}, f32[16,1024]{1,0:T(8,128)}, u32[]{:S(2)}) copy-start(f32[16,1024]{1,0:T(8,128)} %param.19) | copy-start | bytes 196612
  139.1 80.7 %copy-start.26 = (f32[16,1024]{1,0:T(8,128)S(1)}, f32[16,1024]{1,0:T(8,128)}, u32[]{:S(2)}) copy-start(f32[16,1024]{1,0:T(8,128)} %param.18) | copy-start | bytes 196612
  139.2 257.1 %all-gather.10.cloned.1.call-start = ((), (), s32[]{:S(2)}) async-start(), calls=%async_computation.3 | async-start | bytes 1114112 | tf_op jit(solution)/shard_map/all_gather | solution.py:60
  221.4 7.9 %collective-permute-start = (f32[16,1024]{1,0:T(8,128)S(1)}, f32[16,1024]{1,0:T(8,128)S(1)}, u32[]{:S(2)}, u32[]{:S(2)}) collective-permute-start(f32[16,1024]{1,0:T(8,128)S(1)} %get-tuple-element.38), channel_id=1, source_target_pairs={{0,2},{2,4},{4,6},{6,8},{8,10},{10,12},{12,14},{14,16},{16,18},{18... | collective-permute-start | bytes 196616 | tf_op jit(solution)/shard_map/ppermute | solution.py:63
  229.3 8.5 %collective-permute-start.1 = (f32[16,1024]{1,0:T(8,128)S(1)}, f32[16,1024]{1,0:T(8,128)S(1)}, u32[]{:S(2)}, u32[]{:S(2)}) collective-permute-start(f32[16,1024]{1,0:T(8,128)S(1)} %collective-permute-done), channel_id=1, source_target_pairs={{0,2},{2,4},{4,6},{6,8},{8,10},{10,12},{12,14},{14,16},{16,18},{18... | collective-permute-start | bytes 196616 | tf_op jit(solution)/shard_map/ppermute | solution.py:63
  237.8 7.9 %collective-permute-start.2 = (f32[16,1024]{1,0:T(8,128)S(1)}, f32[16,1024]{1,0:T(8,128)S(1)}, u32[]{:S(2)}, u32[]{:S(2)}) collective-permute-start(f32[16,1024]{1,0:T(8,128)S(1)} %collective-permute-done.1), channel_id=1, source_target_pairs={{0,2},{2,4},{4,6},{6,8},{8,10},{10,12},{12,14},{14,16},{16,18},{18... | collective-permute-start | bytes 196616 | tf_op jit(solution)/shard_map/ppermute | solution.py:63
  245.6 7.9 %collective-permute-start.3 = (f32[16,1024]{1,0:T(8,128)S(1)}, f32[16,1024]{1,0:T(8,128)S(1)}, u32[]{:S(2)}, u32[]{:S(2)}) collective-permute-start(f32[16,1024]{1,0:T(8,128)S(1)} %collective-permute-done.2), channel_id=1, source_target_pairs={{0,2},{2,4},{4,6},{6,8},{8,10},{10,12},{12,14},{14,16},{16,18},{18... | collective-permute-start | bytes 196616 | tf_op jit(solution)/shard_map/ppermute | solution.py:63
  253.5 101.6 %copy-start.4 = (f32[16,1024]{1,0:T(8,128)}, f32[16,1024]{1,0:T(8,128)S(1)}, u32[]{:S(2)}) copy-start(f32[16,1024]{1,0:T(8,128)S(1)} %collective-permute-done.3) | copy-start | bytes 196612
  253.5 7.9 %collective-permute-start.4 = (f32[16,1024]{1,0:T(8,128)S(1)}, f32[16,1024]{1,0:T(8,128)S(1)}, u32[]{:S(2)}, u32[]{:S(2)}) collective-permute-start(f32[16,1024]{1,0:T(8,128)S(1)} %collective-permute-done.3), channel_id=1, source_target_pairs={{0,2},{2,4},{4,6},{6,8},{8,10},{10,12},{12,14},{14,16},{16,18},{18... | collective-permute-start | bytes 196616 | tf_op jit(solution)/shard_map/ppermute | solution.py:63
  261.3 78.3 %copy-start.5 = (f32[16,1024]{1,0:T(8,128)}, f32[16,1024]{1,0:T(8,128)S(1)}, u32[]{:S(2)}) copy-start(f32[16,1024]{1,0:T(8,128)S(1)} %collective-permute-done.4) | copy-start | bytes 196612
  261.3 7.9 %collective-permute-start.5 = (f32[16,1024]{1,0:T(8,128)S(1)}, f32[16,1024]{1,0:T(8,128)S(1)}, u32[]{:S(2)}, u32[]{:S(2)}) collective-permute-start(f32[16,1024]{1,0:T(8,128)S(1)} %collective-permute-done.4), channel_id=1, source_target_pairs={{0,2},{2,4},{4,6},{6,8},{8,10},{10,12},{12,14},{14,16},{16,18},{18... | collective-permute-start | bytes 196616 | tf_op jit(solution)/shard_map/ppermute | solution.py:63
  269.2 0.6 copy-start.7
  269.8 7.9 %collective-permute-start.6 = (f32[16,1024]{1,0:T(8,128)S(1)}, f32[16,1024]{1,0:T(8,128)S(1)}, u32[]{:S(2)}, u32[]{:S(2)}) collective-permute-start(f32[16,1024]{1,0:T(8,128)S(1)} %collective-permute-done.5), channel_id=1, source_target_pairs={{0,2},{2,4},{4,6},{6,8},{8,10},{10,12},{12,14},{14,16},{16,18},{18... | collective-permute-start | bytes 196616 | tf_op jit(solution)/shard_map/ppermute | solution.py:63
  278.3 7.9 %collective-permute-start.7 = (f32[16,1024]{1,0:T(8,128)S(1)}, f32[16,1024]{1,0:T(8,128)S(1)}, u32[]{:S(2)}, u32[]{:S(2)}) collective-permute-start(f32[16,1024]{1,0:T(8,128)S(1)} %collective-permute-done.6), channel_id=1, source_target_pairs={{0,2},{2,4},{4,6},{6,8},{8,10},{10,12},{12,14},{14,16},{16,18},{18... | collective-permute-start | bytes 196616 | tf_op jit(solution)/shard_map/ppermute | solution.py:63
  286.2 0.6 copy-start.11
  286.8 7.9 %collective-permute-start.8 = (f32[16,1024]{1,0:T(8,128)S(1)}, f32[16,1024]{1,0:T(8,128)S(1)}, u32[]{:S(2)}, u32[]{:S(2)}) collective-permute-start(f32[16,1024]{1,0:T(8,128)S(1)} %collective-permute-done.7), channel_id=1, source_target_pairs={{0,2},{2,4},{4,6},{6,8},{8,10},{10,12},{12,14},{14,16},{16,18},{18... | collective-permute-start | bytes 196616 | tf_op jit(solution)/shard_map/ppermute | solution.py:63
  294.6 0.6 copy-start.13
  295.3 8.2 %collective-permute-start.9 = (f32[16,1024]{1,0:T(8,128)S(1)}, f32[16,1024]{1,0:T(8,128)S(1)}, u32[]{:S(2)}, u32[]{:S(2)}) collective-permute-start(f32[16,1024]{1,0:T(8,128)S(1)} %collective-permute-done.8), channel_id=1, source_target_pairs={{0,2},{2,4},{4,6},{6,8},{8,10},{10,12},{12,14},{14,16},{16,18},{18... | collective-permute-start | bytes 196616 | tf_op jit(solution)/shard_map/ppermute | solution.py:63
  303.5 0.6 copy-start.15
  304.1 7.9 %collective-permute-start.10 = (f32[16,1024]{1,0:T(8,128)S(1)}, f32[16,1024]{1,0:T(8,128)S(1)}, u32[]{:S(2)}, u32[]{:S(2)}) collective-permute-start(f32[16,1024]{1,0:T(8,128)S(1)} %collective-permute-done.9), channel_id=1, source_target_pairs={{0,2},{2,4},{4,6},{6,8},{8,10},{10,12},{12,14},{14,16},{16,18},{18... | collective-permute-start | bytes 196616 | tf_op jit(solution)/shard_map/ppermute | solution.py:63
  312.0 0.6 copy-start.17
  312.6 7.9 %collective-permute-start.11 = (f32[16,1024]{1,0:T(8,128)S(1)}, f32[16,1024]{1,0:T(8,128)S(1)}, u32[]{:S(2)}, u32[]{:S(2)}) collective-permute-start(f32[16,1024]{1,0:T(8,128)S(1)} %collective-permute-done.10), channel_id=1, source_target_pairs={{0,2},{2,4},{4,6},{6,8},{8,10},{10,12},{12,14},{14,16},{16,18},{18... | collective-permute-start | bytes 196616 | tf_op jit(solution)/shard_map/ppermute | solution.py:63
  320.5 0.6 copy-start.19
  321.1 7.9 %collective-permute-start.12 = (f32[16,1024]{1,0:T(8,128)S(1)}, f32[16,1024]{1,0:T(8,128)S(1)}, u32[]{:S(2)}, u32[]{:S(2)}) collective-permute-start(f32[16,1024]{1,0:T(8,128)S(1)} %collective-permute-done.11), channel_id=1, source_target_pairs={{0,2},{2,4},{4,6},{6,8},{8,10},{10,12},{12,14},{14,16},{16,18},{18... | collective-permute-start | bytes 196616 | tf_op jit(solution)/shard_map/ppermute | solution.py:63
  329.0 0.6 copy-start.21
  329.6 8.0 %collective-permute-start.13 = (f32[16,1024]{1,0:T(8,128)S(1)}, f32[16,1024]{1,0:T(8,128)}, u32[]{:S(2)}, u32[]{:S(2)}) collective-permute-start(f32[16,1024]{1,0:T(8,128)S(1)} %collective-permute-done.12), channel_id=1, source_target_pairs={{0,2},{2,4},{4,6},{6,8},{8,10},{10,12},{12,14},{14,16},{16,18},{18... | collective-permute-start | bytes 196616 | tf_op jit(solution)/shard_map/ppermute | solution.py:63
  337.6 8.2 %collective-permute-start.14 = (f32[16,1024]{1,0:T(8,128)}, f32[16,1024]{1,0:T(8,128)}, u32[]{:S(2)}, u32[]{:S(2)}) collective-permute-start(f32[16,1024]{1,0:T(8,128)} %collective-permute-done.13), channel_id=1, source_target_pairs={{0,2},{2,4},{4,6},{6,8},{8,10},{10,12},{12,14},{14,16},{16,18},{18... | collective-permute-start | bytes 196616 | tf_op jit(solution)/shard_map/ppermute | solution.py:63
  339.6 18.3 %copy-start.2 = (bf16[128,256]{1,0:T(8,128)(2,1)S(1)}, bf16[128,256]{1,0:T(8,128)(2,1)}, u32[]{:S(2)}) copy-start(bf16[128,256]{1,0:T(8,128)(2,1)} %param.17) | copy-start | bytes 196612
  339.6 191.2 %all-gather.12.cloned.1.call-start = ((), (), s32[]{:S(2)}) async-start(), calls=%async_computation.4 | async-start | bytes 4456448 | tf_op jit(solution)/shard_map/all_gather | solution.py:79
  339.7 17.1 %copy-start.22 = (f32[16,1024]{1,0:T(8,128)S(1)}, f32[16,1024]{1,0:T(8,128)}, u32[]{:S(2)}) copy-start(f32[16,1024]{1,0:T(8,128)} %copy-done.21) | copy-start | bytes 196612
  339.7 17.1 %copy-start.20 = (f32[16,1024]{1,0:T(8,128)S(1)}, f32[16,1024]{1,0:T(8,128)}, u32[]{:S(2)}) copy-start(f32[16,1024]{1,0:T(8,128)} %copy-done.19) | copy-start | bytes 196612
  339.7 17.1 %copy-start.18 = (f32[16,1024]{1,0:T(8,128)S(1)}, f32[16,1024]{1,0:T(8,128)}, u32[]{:S(2)}) copy-start(f32[16,1024]{1,0:T(8,128)} %copy-done.17) | copy-start | bytes 196612
  339.7 17.2 %copy-start.16 = (f32[16,1024]{1,0:T(8,128)S(1)}, f32[16,1024]{1,0:T(8,128)}, u32[]{:S(2)}) copy-start(f32[16,1024]{1,0:T(8,128)} %copy-done.15) | copy-start | bytes 196612
  339.7 17.2 %copy-start.14 = (f32[16,1024]{1,0:T(8,128)S(1)}, f32[16,1024]{1,0:T(8,128)}, u32[]{:S(2)}) copy-start(f32[16,1024]{1,0:T(8,128)} %copy-done.13) | copy-start | bytes 196612
  339.7 17.2 %copy-start.12 = (f32[16,1024]{1,0:T(8,128)S(1)}, f32[16,1024]{1,0:T(8,128)}, u32[]{:S(2)}) copy-start(f32[16,1024]{1,0:T(8,128)} %copy-done.11) | copy-start | bytes 196612
  339.8 17.2 %copy-start.10 = (f32[16,1024]{1,0:T(8,128)S(1)}, f32[16,1024]{1,0:T(8,128)}, u32[]{:S(2)}) copy-start(f32[16,1024]{1,0:T(8,128)} %copy-done.9) | copy-start | bytes 196612
  339.8 17.2 %copy-start.8 = (f32[16,1024]{1,0:T(8,128)S(1)}, f32[16,1024]{1,0:T(8,128)}, u32[]{:S(2)}) copy-start(f32[16,1024]{1,0:T(8,128)} %copy-done.7) | copy-start | bytes 196612
  339.8 17.2 %copy-start.6 = (f32[16,1024]{1,0:T(8,128)S(1)}, f32[16,1024]{1,0:T(8,128)}, u32[]{:S(2)}) copy-start(f32[16,1024]{1,0:T(8,128)} %copy-done.5) | copy-start | bytes 196612
  355.1 41.2 %copy-start.3 = (bf16[128,256]{1,0:T(8,128)(2,1)S(1)}, bf16[128,256]{1,0:T(8,128)(2,1)}, u32[]{:S(2)}) copy-start(bf16[128,256]{1,0:T(8,128)(2,1)} %param.16) | copy-start | bytes 196612
  441.4 179.0 %all-gather.14.cloned.1.call-start = ((), (), s32[]{:S(2)}) async-start(), calls=%async_computation.5 | async-start | bytes 4456448 | tf_op jit(solution)/shard_map/all_gather | solution.py:80
  (1 other events, 0.6 us)
Sparse Core Ops, SparseCore 0:
  10.7 57.7 all-gather.5
  71.3 53.9 all-gather.7
  139.3 80.4 reduce-scatter.3
  339.7 56.4 all-gather.9
  441.5 89.3 all-gather.11
  533.4 86.8 all-gather.13
